TPU v7x, 32 devices: a whole 2x2x4 slice. The times are simulated.
32 devices in a mesh: rep: 2 (over y), fs: 4 (over z), tp: 4 (over x, core).
Axes of the slice: x: 2, y: 2, z: 4, core: 2. Of those that a mesh axis runs over, the one named last changes fastest.
Arguments:
- tokens: bfloat16 [4096, 2048], P(('rep', 'fs')), may hold values from -6 to 6
- norm_gain: float32 [2048], replicated, may hold values from 0.1 to 1.9
- gate_weight: bfloat16 [2048, 5632], P('fs', 'tp'), may hold values from -0.125 to 0.125
- up_weight: bfloat16 [2048, 5632], P('fs', 'tp'), may hold values from -0.125 to 0.125
- down_weight: bfloat16 [5632, 2048], P('tp', 'fs'), may hold values from -0.078125 to 0.078125
Outputs:
- branch_out: bfloat16 [4096, 2048], P(('rep', 'fs'))
All inputs are finite; a program needn't handle non-finite values.
Results may differ from a plain program's by a relative error of at most 0.014.
Values may be sent and summed in bfloat16 or wider, within the bound.
A program may use at most 64 MiB of HBM per device.

v0:
```python
import jax
import jax.numpy as jnp
from jax import lax
from jax.sharding import PartitionSpec as P


def add_rows(left, piece):
    return jnp.dot(left, piece, preferred_element_type=jnp.float32)


def per_device(tokens, norm_gain, gate_weight, up_weight, down_weight):
    wide_tok = tokens.astype(jnp.float32)
    scale = lax.rsqrt(jnp.mean(wide_tok * wide_tok, axis=-1, keepdims=True) + 1e-06)
    normed = (wide_tok * scale * norm_gain).astype(jnp.bfloat16)

    def add_one(piece):
        return add_rows(normed, piece)

    gate = add_one(lax.all_gather(gate_weight, "fs", axis=0, tiled=True))
    up = add_one(lax.all_gather(up_weight, "fs", axis=0, tiled=True))
    hidden = (jax.nn.silu(gate) * up).astype(jnp.bfloat16)
    partial_value = jnp.dot(
        hidden,
        lax.all_gather(down_weight, "fs", axis=1, tiled=True),
        preferred_element_type=jnp.float32,
    )
    return lax.psum(partial_value.astype(jnp.bfloat16), "tp")


def solution(mesh):
    in_specs = (P(("rep", "fs"), None), P(), P("fs", "tp"), P("fs", "tp"), P("tp", "fs"))
    out_specs = P(("rep", "fs"), None)
    return jax.shard_map(
        per_device, mesh=mesh, in_specs=in_specs, out_specs=out_specs, check_vma=False
    )
```

profile of v0, /device:TPU:0, one launch (start us, length us, event | category | flops | bytes accessed | tf_op | source)
XLA Modules:
  0.0 404.2 jit_solution(18413360618791287892)
XLA Ops:
  6.5 0.0 copy-start
  6.5 0.0 copy-start.1
  6.5 0.0 all-gather.4.cloned.1.call-start
  6.5 0.7 all-gather.4.cloned.1.call-update
  7.3 0.0 all-gather.6.cloned.1.call-start
  7.3 0.7 all-gather.6.cloned.1.call-update
  8.0 0.0 all-gather.8.cloned.1.call-start
  8.1 0.7 all-gather.8.cloned.1.call-update
  8.7 0.0 all-reduce.2.cloned.1.call-start
  8.8 0.0 copy-done
  8.8 0.5 fusion
  9.3 109.1 %all-gather.4.cloned.1.call-done = bf16[2048,1408]{1,0:T(8,128)(2,1)} async-done(((bf16[512,1408]{1,0:T(8,128)(2,1)}), bf16[2048,1408]{1,0:T(8,128)(2,1)}) %all-gather.4.cloned.1.call-update) | async-done | bytes 5767184 | tf_op jit(solution)/shard_map/all_gather | solution.py:19
  118.3 0.0 copy-done.1
  118.4 7.6 %fusion.6 = f32[512,1408]{1,0:T(8,128)} fusion(bf16[2048,1408]{1,0:T(8,128)(2,1)} %all-gather.4.cloned.1.call-done, bf16[512,2048]{1,0:T(8,128)(2,1)S(1)} %copy-done, f32[2048]{0:T(1024)S(1)} %copy-done.1, f32[512]{0:T(512)S(1)} %add_rsqrt_fusion), kind=kOutput, calls=%fused_computation.8 | convolution fusion | flops 2956984320 | bytes 10758144 | tf_op jit(solution)/shard_map/dot_general | solution.py:8
  126.0 98.9 %all-gather.6.cloned.1.call-done = bf16[2048,1408]{1,0:T(8,128)(2,1)} async-done(((bf16[512,1408]{1,0:T(8,128)(2,1)}), bf16[2048,1408]{1,0:T(8,128)(2,1)}) %all-gather.6.cloned.1.call-update) | async-done | bytes 5767184 | tf_op jit(solution)/shard_map/all_gather | solution.py:20
  224.9 106.5 %all-gather.8.cloned.1.call-done = bf16[1408,2048]{1,0:T(8,128)(2,1)} async-done(((bf16[1408,512]{1,0:T(8,128)(2,1)}), bf16[1408,2048]{1,0:T(8,128)(2,1)}) %all-gather.8.cloned.1.call-update) | async-done | bytes 5767184 | tf_op jit(solution)/shard_map/all_gather | solution.py:24
  331.4 13.3 %convolution_convert_fusion = bf16[512,2048]{1,0:T(8,128)(2,1)} fusion(bf16[1408,2048]{1,0:T(8,128)(2,1)} %all-gather.8.cloned.1.call-done, bf16[2048,1408]{1,0:T(8,128)(2,1)} %all-gather.6.cloned.1.call-done, f32[512,1408]{1,0:T(8,128)} %fusion.6, bf16[512,2048]{1,0:T(8,128)(2,1)S(1)} %copy-done, f32[2048]{0:T(1024)S(1)} %copy-done.1, f32[512]{0:T(512)S(1)} %add_rsqrt_fusion), kind=kOutput, calls=%fused_computation.7 | convolution fusion | flops 5915148288 | bytes 18622464 | tf_op jit(solution)/shard_map/dot_general | solution.py:22
  344.7 0.0 all-reduce.2.cloned.1.call-update
  344.7 49.8 %all-reduce.2.cloned.1.call-done = bf16[512,2048]{1,0:T(8,128)(2,1)} async-done(((bf16[512,2048]{1,0:T(8,128)(2,1)}), bf16[512,2048]{1,0:T(8,128)(2,1)}) %all-reduce.2.cloned.1.call-update) | async-done | bytes 2097168 | tf_op jit(solution)/shard_map/psum | solution.py:27
  394.5 3.2 copy.7
  (1 shorter events, 0.0 us)
Async XLA Ops:
  6.5 2.3 copy-start
  6.5 111.8 %copy-start.1 = (f32[2048]{0:T(1024)S(1)}, f32[2048]{0:T(1024)}, u32[]{:S(2)}) copy-start(f32[2048]{0:T(1024)} %param.6) | copy-start | bytes 24580
  6.5 111.8 %all-gather.4.cloned.1.call-start = ((), (), s32[]{:S(2)}) async-start(), calls=%async_computation | async-start | bytes 7208960 | tf_op jit(solution)/shard_map/all_gather | solution.py:19
  7.3 217.6 %all-gather.6.cloned.1.call-start = ((), (), s32[]{:S(2)}) async-start(), calls=%async_computation.1 | async-start | bytes 7208960 | tf_op jit(solution)/shard_map/all_gather | solution.py:20
  8.0 323.4 %all-gather.8.cloned.1.call-start = ((), (), s32[]{:S(2)}) async-start(), calls=%async_computation.2 | async-start | bytes 7208960 | tf_op jit(solution)/shard_map/all_gather | solution.py:24
  8.7 385.8 %all-reduce.2.cloned.1.call-start = ((), (), s32[]{:S(2)}) async-start(), calls=%async_computation.3 | async-start | bytes 4194304 | tf_op jit(solution)/shard_map/psum | solution.py:27
Sparse Core Ops, SparseCore 0:
  8.9 109.3 all-gather.3
  119.9 104.9 all-gather.5
  226.5 104.9 all-gather.7
  344.9 49.6 all-reduce.1
where the time goes:
time: 404 us
  waiting for transfers between devices  366 us (91%)
  matrix products  20.9 us (5%)
  between operations  13.1 us (3%)
    all_gather x1, waiting for transfers between devices, per_device(): gate = add_one(lax.all_gather(gate_weight, 'fs', axis=0, tiled=True))  109 us
    all_gather x1, waiting for transfers between devices, per_device(): lax.all_gather(down_weight, 'fs', axis=1, tiled=True)  107 us
    all_gather x1, waiting for transfers between devices, per_device(): up = add_one(lax.all_gather(up_weight, 'fs', axis=0, tiled=True))  98.9 us
    psum x1, waiting for transfers between devices, per_device(): return lax.psum(partial_value.astype(jnp.bfloat16), 'tp')  49.8 us
    dot_general x1, matrix products, per_device(): jnp.dot(hidden, lax.all_gather(down_weight, 'fs', axis=1, tiled=True), pr...  13.3 us
  transfers between devices with their start and end apart: 4, of which 4 were waited for; matrix products, arithmetic and copies ran while one was open for 2% of the time, Pallas kernels for 0%

commit v1 on v0

--- a/solution.py
+++ b/solution.py
@@ -24,7 +24,7 @@
         lax.all_gather(down_weight, "fs", axis=1, tiled=True),
         preferred_element_type=jnp.float32,
     )
-    return lax.psum(partial_value.astype(jnp.bfloat16), "tp")
+    return jnp.sum(lax.all_gather(partial_value.astype(jnp.bfloat16), "tp"), axis=0)
 
 
 def solution(mesh):

time: 404 us -> 415 us (1.027)
  other arithmetic: 0.49 us -> 7.69 us
  waiting for transfers between devices: 366 us -> 373 us
    all_gather x0 -> x1, waiting for transfers between devices: none -> 56.7 us  [per_device(): lax.all_gather(partial_value.astype(jnp.bfloat16), 'tp')]
    psum x1 -> x0, waiting for transfers between devices: 49.8 us -> none  [per_device(): return lax.psum(partial_value.astype(jnp.bfloat16), 'tp')]
    all_gather x1, waiting for transfers between devices: 98.9 us -> 107 us  [per_device(): up = add_one(lax.all_gather(up_weight, 'fs', axis=0, tiled=True))]
    all_gather x1, waiting for transfers between devices: 107 us -> 98.9 us  [per_device(): lax.all_gather(down_weight, 'fs', axis=1, tiled=True)]
    reduce_sum x0 -> x1, other arithmetic: none -> 7.2 us  [per_device(): jnp.sum(lax.all_gather(partial_value.astype(jnp.bfloat16), 'tp'), axis=0)]
where the time goes in v1:
time: 415 us
  waiting for transfers between devices  373 us (90%)
  matrix products  20.9 us (5%)
  between operations  13.1 us (3%)
  other arithmetic  7.69 us (2%)
    all_gather x1, waiting for transfers between devices, per_device(): gate = add_one(lax.all_gather(gate_weight, 'fs', axis=0, tiled=True))  109 us
    all_gather x1, waiting for transfers between devices, per_device(): up = add_one(lax.all_gather(up_weight, 'fs', axis=0, tiled=True))  107 us
    all_gather x1, waiting for transfers between devices, per_device(): lax.all_gather(down_weight, 'fs', axis=1, tiled=True)  98.9 us
    all_gather x1, waiting for transfers between devices, per_device(): lax.all_gather(partial_value.astype(jnp.bfloat16), 'tp')  56.7 us
    dot_general x1, matrix products, per_device(): jnp.dot(hidden, lax.all_gather(down_weight, 'fs', axis=1, tiled=True), pr...  13.3 us
  transfers between devices with their start and end apart: 4, of which 4 were waited for; matrix products, arithmetic and copies ran while one was open for 2% of the time, Pallas kernels for 0%

profile of v1, /device:TPU:0, one launch (start us, length us, event | category | flops | bytes accessed | tf_op | source)
XLA Modules:
  0.0 415.2 jit_solution(5861046165614172538)
XLA Ops:
  6.5 0.0 copy-start
  6.5 0.0 copy-start.1
  6.5 0.0 all-gather.6.cloned.1.call-start
  6.5 0.7 all-gather.6.cloned.1.call-update
  7.3 0.0 all-gather.10.cloned.1.call-start
  7.3 0.7 all-gather.10.cloned.1.call-update
  8.0 0.0 all-gather.8.cloned.1.call-start
  8.1 0.7 all-gather.8.cloned.1.call-update
  8.7 0.0 all-gather.12.cloned.1.call-start
  8.8 0.0 copy-done
  8.8 0.5 fusion
  9.3 109.1 %all-gather.6.cloned.1.call-done = bf16[2048,1408]{1,0:T(8,128)(2,1)} async-done(((bf16[512,1408]{1,0:T(8,128)(2,1)}), bf16[2048,1408]{1,0:T(8,128)(2,1)}) %all-gather.6.cloned.1.call-update) | async-done | bytes 5767184 | tf_op jit(solution)/shard_map/all_gather | solution.py:19
  118.3 0.0 copy-done.1
  118.4 7.6 %fusion.6 = f32[512,1408]{1,0:T(8,128)} fusion(bf16[2048,1408]{1,0:T(8,128)(2,1)} %all-gather.6.cloned.1.call-done, bf16[512,2048]{1,0:T(8,128)(2,1)S(1)} %copy-done, f32[2048]{0:T(1024)S(1)} %copy-done.1, f32[512]{0:T(512)S(1)} %add_rsqrt_fusion), kind=kOutput, calls=%fused_computation.8 | convolution fusion | flops 2956984320 | bytes 10758144 | tf_op jit(solution)/shard_map/dot_general | solution.py:8
  126.0 98.9 %all-gather.10.cloned.1.call-done = bf16[1408,2048]{1,0:T(8,128)(2,1)} async-done(((bf16[1408,512]{1,0:T(8,128)(2,1)}), bf16[1408,2048]{1,0:T(8,128)(2,1)}) %all-gather.10.cloned.1.call-update) | async-done | bytes 5767184 | tf_op jit(solution)/shard_map/all_gather | solution.py:24
  224.9 106.5 %all-gather.8.cloned.1.call-done = bf16[2048,1408]{1,0:T(8,128)(2,1)} async-done(((bf16[512,1408]{1,0:T(8,128)(2,1)}), bf16[2048,1408]{1,0:T(8,128)(2,1)}) %all-gather.8.cloned.1.call-update) | async-done | bytes 5767184 | tf_op jit(solution)/shard_map/all_gather | solution.py:20
  331.4 13.3 %convolution_convert_fusion = bf16[512,2048]{1,0:T(8,128)(2,1)} fusion(bf16[1408,2048]{1,0:T(8,128)(2,1)} %all-gather.10.cloned.1.call-done, bf16[2048,1408]{1,0:T(8,128)(2,1)} %all-gather.8.cloned.1.call-done, f32[512,1408]{1,0:T(8,128)} %fusion.6, bf16[512,2048]{1,0:T(8,128)(2,1)S(1)} %copy-done, f32[2048]{0:T(1024)S(1)} %copy-done.1, ...), kind=kOutput, calls=%fused_computation.7 | convolution fusion | flops 5915148288 | bytes 18622464 | tf_op jit(solution)/shard_map/dot_general | solution.py:22
  344.7 0.0 all-gather.12.cloned.1.call-update
  344.8 56.7 %all-gather.12.cloned.1.call-done = bf16[2048,2048]{1,0:T(8,128)(2,1)} async-done(((bf16[512,2048]{1,0:T(8,128)(2,1)}), bf16[2048,2048]{1,0:T(8,128)(2,1)}) %all-gather.12.cloned.1.call-update) | async-done | bytes 8388624 | tf_op jit(solution)/shard_map/all_gather | solution.py:27
  401.4 7.2 %reduce_sum.22 = bf16[512,2048]{1,0:T(8,128)(2,1)} reduce(bf16[4,512,2048]{2,1,0:T(8,128)(2,1)} %bitcast.4, bf16[]{:T(256)} %constant.11.clone.1), dimensions={0}, to_apply=%region_1.2 | reduce | flops 3145728 | bytes 10485762 | tf_op jit(solution)/shard_map/reduce_sum | solution.py:27
  (1 shorter events, 0.0 us)
Async XLA Ops:
  6.5 2.3 copy-start
  6.5 111.8 %copy-start.1 = (f32[2048]{0:T(1024)S(1)}, f32[2048]{0:T(1024)}, u32[]{:S(2)}) copy-start(f32[2048]{0:T(1024)} %param.6) | copy-start | bytes 24580
  6.5 111.8 %all-gather.6.cloned.1.call-start = ((), (), s32[]{:S(2)}) async-start(), calls=%async_computation | async-start | bytes 7208960 | tf_op jit(solution)/shard_map/all_gather | solution.py:19
  7.3 217.6 %all-gather.10.cloned.1.call-start = ((), (), s32[]{:S(2)}) async-start(), calls=%async_computation.2 | async-start | bytes 7208960 | tf_op jit(solution)/shard_map/all_gather | solution.py:24
  8.0 323.4 %all-gather.8.cloned.1.call-start = ((), (), s32[]{:S(2)}) async-start(), calls=%async_computation.1 | async-start | bytes 7208960 | tf_op jit(solution)/shard_map/all_gather | solution.py:20
  8.7 392.7 %all-gather.12.cloned.1.call-start = ((), (), s32[]{:S(2)}) async-start(), calls=%async_computation.3 | async-start | bytes 10485760 | tf_op jit(solution)/shard_map/all_gather | solution.py:27
Sparse Core Ops, SparseCore 0:
  8.9 109.3 all-gather.5
  119.9 104.9 all-gather.9
  226.5 104.9 all-gather.7
  344.9 56.5 all-gather.11

commit v2 on v0

--- a/solution.py
+++ b/solution.py
@@ -21,7 +21,7 @@
     hidden = (jax.nn.silu(gate) * up).astype(jnp.bfloat16)
     partial_value = jnp.dot(
         hidden,
-        lax.all_gather(down_weight, "fs", axis=1, tiled=True),
+        jnp.concatenate(lax.all_gather(down_weight, "fs"), axis=1),
         preferred_element_type=jnp.float32,
     )
     return lax.psum(partial_value.astype(jnp.bfloat16), "tp")

time: 404 us -> 405 us (level)
  local copies, waits for them, and re-layouts: 3.17 us -> 11.6 us
  waiting for transfers between devices: 366 us -> 358 us
    all_gather x1, waiting for transfers between devices: 109 us -> 98.1 us  [per_device(): gate = add_one(lax.all_gather(gate_weight, 'fs', axis=0, tiled=True))]
    reshape x0 -> x1, local copies, waits for them, and re-layouts: none -> 8.46 us  [per_device(): jnp.concatenate(lax.all_gather(down_weight, 'fs'), axis=1)]
  transfers between devices with their start and end apart: 4 -> 4, of which waited for: 4 -> 4; matrix products, arithmetic and copies ran while one was open for 2% -> 4% of each run, Pallas kernels for 0% -> 0%
where the time goes in v2:
time: 405 us; the launch traced here: 404 us
  waiting for transfers between devices  358 us (88%)
  matrix products  20.9 us (5%)
  between operations  13.1 us (3%)
  local copies, waits for them, and re-layouts  11.6 us (3%)
    all_gather x1, waiting for transfers between devices, per_device(): lax.all_gather(down_weight, 'fs')  109 us
    all_gather x1, waiting for transfers between devices, per_device(): up = add_one(lax.all_gather(up_weight, 'fs', axis=0, tiled=True))  98.9 us
    all_gather x1, waiting for transfers between devices, per_device(): gate = add_one(lax.all_gather(gate_weight, 'fs', axis=0, tiled=True))  98.1 us
    psum x1, waiting for transfers between devices, per_device(): return lax.psum(partial_value.astype(jnp.bfloat16), 'tp')  49.8 us
    dot_general x1, matrix products, per_device(): jnp.dot(hidden, jnp.concatenate(lax.all_gather(down_weight, 'fs'), axis=1...  13.3 us
    reshape x1, local copies, waits for them, and re-layouts, per_device(): jnp.concatenate(lax.all_gather(down_weight, 'fs'), axis=1)  8.46 us
  transfers between devices with their start and end apart: 4, of which 4 were waited for; matrix products, arithmetic and copies ran while one was open for 4% of the time, Pallas kernels for 0%

profile of v2, /device:TPU:0, one launch (start us, length us, event | category | flops | bytes accessed | tf_op | source)
XLA Modules:
  0.0 404.2 jit_solution(311619322179481045)
XLA Ops:
  6.5 0.0 copy-start
  6.5 0.0 all-gather.9.cloned.1.call-start
  6.5 0.7 all-gather.9.cloned.1.call-update
  7.3 0.0 all-gather.5.cloned.1.call-start
  7.3 0.7 all-gather.5.cloned.1.call-update
  8.0 0.0 all-gather.7.cloned.1.call-start
  8.1 0.7 all-gather.7.cloned.1.call-update
  8.7 0.0 all-reduce.2.cloned.1.call-start
  8.8 0.0 copy-done
  8.8 0.5 fusion
  9.3 109.1 %all-gather.9.cloned.1.call-done = bf16[5632,512]{1,0:T(8,128)(2,1)} async-done(((bf16[1408,512]{1,0:T(8,128)(2,1)}), bf16[5632,512]{1,0:T(8,128)(2,1)}) %all-gather.9.cloned.1.call-update) | async-done | bytes 5767184 | tf_op jit(solution)/shard_map/all_gather | solution.py:24
  118.3 0.0 copy-start.1
  118.3 8.5 %copy.6 = bf16[1408,4,512]{0,2,1:T(8,128)(2,1)} copy(bf16[1408,4,512]{2,0,1:T(8,128)(2,1)} %bitcast.7) | data formatting | bytes 11534336 | tf_op jit(solution)/shard_map/reshape | solution.py:24
  126.8 98.1 %all-gather.5.cloned.1.call-done = bf16[2048,1408]{1,0:T(8,128)(2,1)} async-done(((bf16[512,1408]{1,0:T(8,128)(2,1)}), bf16[2048,1408]{1,0:T(8,128)(2,1)}) %all-gather.5.cloned.1.call-update) | async-done | bytes 5767184 | tf_op jit(solution)/shard_map/all_gather | solution.py:19
  224.9 0.0 copy-done.1
  224.9 7.6 %fusion.6 = f32[512,1408]{1,0:T(8,128)} fusion(bf16[2048,1408]{1,0:T(8,128)(2,1)} %all-gather.5.cloned.1.call-done, bf16[512,2048]{1,0:T(8,128)(2,1)S(1)} %copy-done, f32[2048]{0:T(1024)S(1)} %copy-done.1, f32[512]{0:T(512)S(1)} %add_rsqrt_fusion), kind=kOutput, calls=%fused_computation.8 | convolution fusion | flops 2956984320 | bytes 10758144 | tf_op jit(solution)/shard_map/dot_general | solution.py:8
  232.5 98.9 %all-gather.7.cloned.1.call-done = bf16[2048,1408]{1,0:T(8,128)(2,1)} async-done(((bf16[512,1408]{1,0:T(8,128)(2,1)}), bf16[2048,1408]{1,0:T(8,128)(2,1)}) %all-gather.7.cloned.1.call-update) | async-done | bytes 5767184 | tf_op jit(solution)/shard_map/all_gather | solution.py:20
  331.4 13.3 %convolution_convert_fusion = bf16[512,2048]{1,0:T(8,128)(2,1)} fusion(bf16[1408,2048]{0,1:T(8,128)(2,1)} %bitcast.8, bf16[2048,1408]{1,0:T(8,128)(2,1)} %all-gather.7.cloned.1.call-done, f32[512,1408]{1,0:T(8,128)} %fusion.6, bf16[512,2048]{1,0:T(8,128)(2,1)S(1)} %copy-done, f32[2048]{0:T(1024)S(1)} %copy-done.1, f32[512]{0:T(512)S(1)} %add_rsqrt_fusion), kind=kOutput, calls=%fused_computation.7 | convolution fusion | flops 5915148288 | bytes 18622464 | tf_op jit(solution)/shard_map/dot_general | solution.py:22
  344.7 0.0 all-reduce.2.cloned.1.call-update
  344.7 49.8 %all-reduce.2.cloned.1.call-done = bf16[512,2048]{1,0:T(8,128)(2,1)} async-done(((bf16[512,2048]{1,0:T(8,128)(2,1)}), bf16[512,2048]{1,0:T(8,128)(2,1)}) %all-reduce.2.cloned.1.call-update) | async-done | bytes 2097168 | tf_op jit(solution)/shard_map/psum | solution.py:27
  394.5 3.2 copy.8
  (1 shorter events, 0.0 us)
Async XLA Ops:
  6.5 2.3 copy-start
  6.5 111.8 %all-gather.9.cloned.1.call-start = ((), (), s32[]{:S(2)}) async-start(), calls=%async_computation.3 | async-start | bytes 7208960 | tf_op jit(solution)/shard_map/all_gather | solution.py:24
  7.3 217.6 %all-gather.5.cloned.1.call-start = ((), (), s32[]{:S(2)}) async-start(), calls=%async_computation | async-start | bytes 7208960 | tf_op jit(solution)/shard_map/all_gather | solution.py:19
  8.0 323.4 %all-gather.7.cloned.1.call-start = ((), (), s32[]{:S(2)}) async-start(), calls=%async_computation.1 | async-start | bytes 7208960 | tf_op jit(solution)/shard_map/all_gather | solution.py:20
  8.7 385.8 %all-reduce.2.cloned.1.call-start = ((), (), s32[]{:S(2)}) async-start(), calls=%async_computation.2 | async-start | bytes 4194304 | tf_op jit(solution)/shard_map/psum | solution.py:27
  118.3 106.5 %copy-start.1 = (f32[2048]{0:T(1024)S(1)}, f32[2048]{0:T(1024)}, u32[]{:S(2)}) copy-start(f32[2048]{0:T(1024)} %param.6) | copy-start | bytes 24580
Sparse Core Ops, SparseCore 0:
  8.9 109.3 all-gather.8
  119.9 104.9 all-gather.4
  226.5 104.9 all-gather.6
  344.8 49.6 all-reduce.1
